TPU v7x, 32 devices: a whole 2x2x4 slice. The times are simulated.
32 devices in a mesh: grp: 2 (over y), tp: 4 (over z), dp: 4 (over x, core).
Axes of the slice: x: 2, y: 2, z: 4, core: 2. Of those that a mesh axis runs over, the one named last changes fastest.
Arguments:
- stream: bfloat16 [256, 4096], P(('grp', 'tp'), 'dp'), parts along dimension 0, may hold values from -6 to 6
- lengths: int32 [16], P(('grp', 'dp')), parts along dimension 0, may hold values from 1 to 16, as said below
- input_norm_gain: float32 [2, 4096], P(None, 'dp'), may hold values from 0.1 to 1.9
- query_projection: bfloat16 [2, 4096, 2048], P(None, 'dp', 'tp'), may hold values from -0.09375 to 0.09375
- key_projection: bfloat16 [2, 4096, 2048], P(None, 'dp', 'tp'), may hold values from -0.09375 to 0.09375
- forget_gate_weight: bfloat16 [2, 4096, 2048], P(None, 'dp', 'tp'), may hold values from -0.09375 to 0.09375
- value_projection: bfloat16 [2, 4096, 4096], P(None, 'dp', 'tp'), may hold values from -0.09375 to 0.09375
- output_gate_weight: bfloat16 [2, 4096, 4096], P(None, 'dp', 'tp'), may hold values from -0.09375 to 0.09375
- forget_gate_bias: float32 [2, 2048], P(None, 'tp'), may hold values from -3 to 3
- extra_frame_decay: float32 [2, 256, 2048], P(None, ('grp', 'dp'), 'tp'), parts along dimension 1, may hold values from -0.7 to 0, as said below
- head_norm_gain: float32 [2, 512], replicated, may hold values from 0.1 to 1.9
- output_projection: bfloat16 [2, 4096, 4096], P(None, 'tp', 'dp'), may hold values from -0.09375 to 0.09375
- memory: float32 [2, 16, 2048, 512], P(None, ('grp', 'dp'), 'tp'), parts along dimension 1, may hold values from -6 to 6
Outputs:
- stream_out: bfloat16 [256, 4096], P(('grp', 'tp'), 'dp'), parts along dimension 0
- memory_out: float32 [2, 16, 2048, 512], P(None, ('grp', 'dp'), 'tp'), parts along dimension 1
There are 2 independent parts, one for each index of `grp`. A program takes and returns all parts, laid end to end along the dimension named above; an argument that names none is the same for every part. Nothing has to cross between parts.
Inputs may be any that keep to these rules, and one draw needn't show every extreme that they name: `lengths`: live frames of each sequence; at least one sequence has all 16. `extra_frame_decay`: zero at most frames; at the others, for every key channel, a value from -0.7 to -0.22.
All inputs are finite; a program needn't handle non-finite values.
Results may differ from a plain program's by a relative error of at most 0.03.
Values may be sent and summed in bfloat16 or wider, within the bound.
A program may use at most 64 MiB of HBM per device.

v0:
```python
import jax
import jax.numpy as jnp
from jax import lax
from jax.sharding import PartitionSpec as P

D = 4096
KEY_DIM = 256
VALUE_DIM = 512
BLOCK_LEN = 16


EPS = 1e-06
TIME_CONSTANT = 16.0
HIGH = lax.Precision.HIGHEST


def for_sending(array):
    return jax.tree.map(lambda a: a.astype(jnp.bfloat16) if a.dtype == jnp.float32 else a, array)


def swapped(value, axis, distance):
    mask = 2**distance
    pairs = [(source, source ^ mask) for source in range(lax.axis_size(axis))]
    return lax.ppermute(value, axis, pairs)


def recurrence(queries, keys_in, values_in, decay_logarithm, state_in):
    frames = queries.shape[1]
    totals = jnp.cumsum(decay_logarithm, axis=1)
    causal = (jnp.arange(frames)[:, None] >= jnp.arange(frames)[None, :])[None, :, :, None, None]
    spread = totals[:, :, None] - totals[:, None, :]
    decays = jnp.where(causal, jnp.exp(jnp.where(causal, spread, 0.0)), 0.0)
    scores = jnp.einsum("sihk,sijhk,sjhk->shij", queries, decays, keys_in, precision=HIGH)
    inner_part = jnp.einsum("shij,sjhv->sihv", scores, values_in, precision=HIGH)
    carried = jnp.einsum("sihk,shkv->sihv", queries * jnp.exp(totals), state_in, precision=HIGH)
    last_total = totals[:, -1]
    weighted = keys_in * jnp.exp(last_total[:, None] - totals)
    fresh_mem = jnp.exp(last_total)[..., None] * state_in + jnp.einsum(
        "sjhk,sjhv->shkv", weighted, values_in, precision=HIGH
    )
    return (inner_part + carried, fresh_mem)


def local(
    stream,
    lengths,
    input_norm_gain,
    query_projection,
    key_projection,
    forget_gate_weight,
    value_projection,
    output_gate_weight,
    forget_gate_bias,
    extra_frame_decay,
    head_norm_gain,
    output_projection,
    memory,
):
    key_local = query_projection.shape[2]
    value_local = value_projection.shape[2]
    local_heads = max(1, key_local // KEY_DIM)
    key_width = key_local // local_heads
    paired = key_local < KEY_DIM
    seq_local = lengths.shape[0]
    own_tokens = seq_local * BLOCK_LEN
    tp_spot = lax.axis_index("tp")
    position = jnp.arange(BLOCK_LEN, dtype=jnp.int32)
    alive_mask = (position[None, :] < lengths[:, None]).astype(jnp.float32).reshape(own_tokens, 1)
    current = stream
    outputs = []
    for block_layer in range(2):
        residual = current.astype(jnp.float32)
        gathered = lax.all_gather(current, "tp", axis=0, tiled=True)
        wide_res = gathered.astype(jnp.float32)
        scaled = (wide_res * input_norm_gain[block_layer]).astype(jnp.bfloat16)
        own_power = lax.psum_scatter(
            jnp.sum(wide_res * wide_res, axis=1), "dp", scatter_dimension=0, tiled=True
        )
        row_scale = lax.rsqrt(own_power / D + EPS)[:, None]
        joined = jnp.concatenate(
            [
                query_projection[block_layer],
                key_projection[block_layer],
                forget_gate_weight[block_layer],
                value_projection[block_layer],
                output_gate_weight[block_layer],
            ],
            axis=1,
        )
        summed = (
            lax.psum_scatter(
                jnp.dot(scaled, joined, preferred_element_type=jnp.float32).astype(jnp.bfloat16),
                "dp",
                scatter_dimension=0,
                tiled=True,
            ).astype(jnp.float32)
            * row_scale
        )
        second_cut = 2 * key_local
        third_cut = 3 * key_local
        fourth_cut = 3 * key_local + value_local
        queries = summed[:, :key_local] * KEY_DIM ** (-0.5)
        keys_in = summed[:, key_local:second_cut] * alive_mask
        forget_preactivation = summed[:, second_cut:third_cut] + forget_gate_bias[block_layer]
        values_in = summed[:, third_cut:fourth_cut]
        gate_pre = summed[:, fourth_cut:]
        decay_logarithm = (
            jax.nn.log_sigmoid(forget_preactivation) / TIME_CONSTANT
            + extra_frame_decay[block_layer]
        ) * alive_mask
        is_upper = tp_spot % 2 == 1
        if paired:
            partner = swapped(for_sending(values_in), "tp", 0).astype(values_in.dtype)
            values_full = jnp.where(
                is_upper,
                jnp.concatenate([partner, values_in], 1),
                jnp.concatenate([values_in, partner], 1),
            )
        else:
            values_full = values_in
        read_out, fresh_mem = recurrence(
            queries.reshape(seq_local, BLOCK_LEN, local_heads, key_width),
            keys_in.reshape(seq_local, BLOCK_LEN, local_heads, key_width),
            values_full.reshape(seq_local, BLOCK_LEN, local_heads, VALUE_DIM),
            decay_logarithm.reshape(seq_local, BLOCK_LEN, local_heads, key_width),
            memory[block_layer].reshape(seq_local, local_heads, key_width, VALUE_DIM),
        )
        if paired:
            read_out = read_out + swapped(for_sending(read_out), "tp", 0).astype(read_out.dtype)
        normed = (
            read_out
            * lax.rsqrt(jnp.mean(read_out * read_out, axis=3, keepdims=True) + EPS)
            * head_norm_gain[block_layer]
        )
        flat = normed.reshape(own_tokens, local_heads * VALUE_DIM)
        if paired:
            flat = lax.dynamic_slice_in_dim(flat, tp_spot % 2 * value_local, value_local, 1)
        gated = (flat * jax.nn.silu(gate_pre) * alive_mask).astype(jnp.bfloat16)
        partials = jnp.dot(
            lax.all_gather(gated, "dp", axis=0, tiled=True),
            output_projection[block_layer],
            preferred_element_type=jnp.float32,
        )
        mixer_out = lax.psum_scatter(
            partials.astype(jnp.bfloat16), "tp", scatter_dimension=0, tiled=True
        )
        current = (residual + mixer_out.astype(jnp.float32)).astype(jnp.bfloat16)
        outputs.append(fresh_mem.reshape(seq_local, key_local, VALUE_DIM))
    return (current, jnp.stack(outputs))


def solution(mesh):
    placed = (
        P(("grp", "tp"), "dp"),
        P(("grp", "dp")),
        P(None, "dp"),
        P(None, "dp", "tp"),
        P(None, "dp", "tp"),
        P(None, "dp", "tp"),
        P(None, "dp", "tp"),
        P(None, "dp", "tp"),
        P(None, "tp"),
        P(None, ("grp", "dp"), "tp"),
        P(),
        P(None, "tp", "dp"),
        P(None, ("grp", "dp"), "tp", None),
    )
    return jax.shard_map(
        local,
        mesh=mesh,
        in_specs=placed,
        out_specs=(P(("grp", "tp"), "dp"), P(None, ("grp", "dp"), "tp", None)),
        check_vma=False,
    )
```

profile of v0, /device:TPU:0, one launch (start us, length us, event | category | flops | bytes accessed | tf_op | source)
XLA Modules:
  0.0 178.1 jit_solution(17307590253444352245)
XLA Ops:
  7.3 1.8 %bitcast_dynamic-update-slice_fusion.9 = (bf16[1024,3584]{1,0:T(8,128)(2,1)S(1)}, bf16[1024,3584]{1,0:T(8,128)(2,1)S(1)}) fusion(bf16[2,1024,512]{2,1,0:T(8,128)(2,1)} %param.16), kind=kLoop, calls=%fused_computation.28 | loop fusion | bytes 4194304
  9.1 15.8 %all_gather.12 = bf16[128,1024]{1,0:T(8,128)(2,1)S(1)} all-gather(bf16[32,1024]{1,0:T(8,128)(2,1)S(1)} %copy-done.6), channel_id=1, replica_groups=mesh['grp'=2,'tp'=4,'dp'=4] {'tp'}, dimensions={0}, use_global_device_ids=true | all-gather | bytes 327680 | tf_op jit(solution)/shard_map/all_gather | solution.py:73
  25.2 1.9 %copy-done.2 = bf16[2,1024,1024]{2,1,0:T(8,128)(2,1)S(1)} copy-done((bf16[2,1024,1024]{2,1,0:T(8,128)(2,1)S(1)}, bf16[2,1024,1024]{2,1,0:T(8,128)(2,1)}, u32[]{:S(2)}) %copy-start.2) | copy-done | bytes 4194328
  27.5 1.7 copy-done.3
  29.7 2.9 %copy-done = bf16[1024,3584]{1,0:T(8,128)(2,1)} copy-done((bf16[1024,3584]{1,0:T(8,128)(2,1)}, bf16[1024,3584]{1,0:T(8,128)(2,1)S(1)}, u32[]{:S(2)}) %copy-start) | copy-done | bytes 7340056
  32.7 2.1 %convolution_convert_fusion.1 = bf16[128,3584]{1,0:T(8,128)(2,1)} fusion(bf16[1024,3584]{1,0:T(8,128)(2,1)S(1)} %get-tuple-element.2, bf16[128,1024]{1,0:T(8,128)(2,1)S(1)} %all_gather.12, f32[1024]{0:T(1024)S(1)} %bitcast.102), kind=kOutput, calls=%fused_computation.1 | convolution fusion | flops 940376064 | bytes 8523776 | tf_op jit(solution)/shard_map/dot_general | solution.py:92
  36.4 5.7 %all-reduce = f32[128]{0:T(128)S(1)} all-reduce(f32[128]{0:T(128)S(1)} %fusion.19), channel_id=3, replica_groups=mesh['grp'=2,'tp'=4,'dp'=4] {'dp'}, use_global_device_ids=true, to_apply=%region_2.0.clone | all-reduce | flops 128 | bytes 1024
  42.2 4.3 %fusion.52 = (f32[1,2,512,512]{3,2,1,0:T(8,128)}, f32[1,2,512,512]{3,2,1,0:T(8,128)S(1)}) fusion(f32[2,2,512,512]{3,2,1,0:T(8,128)} %param.25), kind=kLoop, calls=%fused_computation.101 | loop fusion | bytes 8388608 | tf_op jit(solution)/shard_map/slice | solution.py:126
  46.5 14.1 %reduce-scatter.5.cloned.1.call-done = bf16[32,3584]{1,0:T(8,128)(2,1)} async-done(((bf16[128,3584]{1,0:T(8,128)(2,1)}), bf16[32,3584]{1,0:T(8,128)(2,1)}) %reduce-scatter.5.cloned.1.call-update) | async-done | bytes 229392 | tf_op jit(solution)/shard_map/reduce_scatter | solution.py:91
  60.5 1.0 convert_multiply_fusion.5
  62.1 1.1 multiply_bitcast_fusion.1
  63.3 2.8 %convolution_bitcast_fusion.2 = f32[2,16,2,512]{3,1,2,0:T(8,128)S(1)} fusion(f32[2,2,256,512]{3,2,1,0:T(8,128)} %bitcast.91, f32[2,16,2,256]{3,2,1,0:T(2,128)S(1)} %get-tuple-element.21), kind=kOutput, calls=%fused_computation.20 | convolution fusion | flops 100663296 | bytes 2293760 | tf_op jit(solution)/shard_map/sihk,shkv->sihv/dot_general | solution.py:35
  66.0 1.0 fusion.16
  67.7 5.8 %all_gather.13 = bf16[128,1024]{1,0:T(8,128)(2,1)S(1)} all-gather(bf16[32,1024]{1,0:T(8,128)(2,1)S(1)} %multiply_convert_fusion.1), channel_id=1, replica_groups=mesh['grp'=2,'tp'=4,'dp'=4] {'dp'}, dimensions={0}, use_global_device_ids=true | all-gather | bytes 327680 | tf_op jit(solution)/shard_map/all_gather | solution.py:140
  73.5 1.1 fusion.6
  74.7 20.1 %reduce-scatter.7.cloned.1.call-done = bf16[32,1024]{1,0:T(8,128)(2,1)} async-done(((bf16[128,1024]{1,0:T(8,128)(2,1)}), bf16[32,1024]{1,0:T(8,128)(2,1)}) %reduce-scatter.7.cloned.1.call-update) | async-done | bytes 65552 | tf_op jit(solution)/shard_map/reduce_scatter | solution.py:144
  94.8 0.9 add_convert_fusion.1
  95.7 14.0 %all_gather.14 = bf16[128,1024]{1,0:T(8,128)(2,1)S(1)} all-gather(bf16[32,1024]{1,0:T(8,128)(2,1)S(1)} %add_convert_fusion.1), channel_id=1, replica_groups=mesh['grp'=2,'tp'=4,'dp'=4] {'tp'}, dimensions={0}, use_global_device_ids=true | all-gather | bytes 327680 | tf_op jit(solution)/shard_map/all_gather | solution.py:73
  109.7 5.2 %convolution_convert_fusion = bf16[128,3584]{1,0:T(8,128)(2,1)} fusion(bf16[1024,3584]{1,0:T(8,128)(2,1)} %copy-done, bf16[128,1024]{1,0:T(8,128)(2,1)S(1)} %all_gather.14, f32[1024]{0:T(1024)S(1)} %bitcast.101), kind=kOutput, calls=%fused_computation | convolution fusion | flops 940376064 | bytes 8523776 | tf_op jit(solution)/shard_map/dot_general | solution.py:92
  114.9 4.8 %multiply_add_fusion.1 = f32[2,2,256,512]{3,2,1,0:T(8,128)} fusion(f32[2,2,256,512]{3,2,1,0:T(8,128)} %bitcast.92, f32[2,2,256]{2,1,0:T(2,128)S(1)} %fusion.50, f32[2,16,2,512]{3,2,1,0:T(2,128)S(1)} %reshape.100, f32[2,16,2,256]{3,2,1,0:T(2,128)S(1)} %get-tuple-element.20), kind=kOutput, calls=%fused_computation.12 | convolution fusion | flops 101711872 | bytes 4395008 | tf_op jit(solution)/shard_map/sjhk,sjhv->shkv/dot_general | solution.py:38
  119.9 5.8 %all-reduce.1 = f32[128]{0:T(128)S(1)} all-reduce(f32[128]{0:T(128)S(1)} %fusion.21), channel_id=6, replica_groups=mesh['grp'=2,'tp'=4,'dp'=4] {'dp'}, use_global_device_ids=true, to_apply=%region_8.9.clone | all-reduce | flops 128 | bytes 1024
  125.8 11.7 %reduce-scatter.9.cloned.1.call-done = bf16[32,3584]{1,0:T(8,128)(2,1)} async-done(((bf16[128,3584]{1,0:T(8,128)(2,1)}), bf16[32,3584]{1,0:T(8,128)(2,1)}) %reduce-scatter.9.cloned.1.call-update) | async-done | bytes 229392 | tf_op jit(solution)/shard_map/reduce_scatter | solution.py:91
  137.4 1.0 convert_multiply_fusion.4
  139.0 1.1 multiply_bitcast_fusion
  140.2 1.0 fusion.14
  141.2 1.1 convolution_bitcast_fusion
  142.9 5.8 %all_gather.15 = bf16[128,1024]{1,0:T(8,128)(2,1)S(1)} all-gather(bf16[32,1024]{1,0:T(8,128)(2,1)S(1)} %multiply_convert_fusion), channel_id=1, replica_groups=mesh['grp'=2,'tp'=4,'dp'=4] {'dp'}, dimensions={0}, use_global_device_ids=true | all-gather | bytes 327680 | tf_op jit(solution)/shard_map/all_gather | solution.py:140
  148.7 1.2 fusion.9
  149.9 1.9 %multiply_add_fusion = f32[2,2,256,512]{3,2,1,0:T(8,128)S(1)} fusion(f32[2,2,256,512]{3,2,1,0:T(8,128)S(1)} %bitcast.90, f32[2,2,256]{2,1,0:T(2,128)S(1)} %fusion.51, f32[2,16,2,512]{3,2,1,0:T(2,128)S(1)} %reshape.105, f32[2,16,2,256]{3,2,1,0:T(2,128)S(1)} %get-tuple-element.22), kind=kOutput, calls=%fused_computation.11 | convolution fusion | flops 101711872 | bytes 4395008 | tf_op jit(solution)/shard_map/sjhk,sjhv->shkv/dot_general | solution.py:38
  151.8 2.5 %pad_maximum_fusion = f32[2,2,512,512]{3,2,1,0:T(8,128)} fusion(f32[1,2,512,512]{3,2,1,0:T(8,128)S(1)} %bitcast.94, f32[1,2,512,512]{3,2,1,0:T(8,128)S(1)} %bitcast.93), kind=kLoop, calls=%fused_computation.2 | loop fusion | flops 1048576 | bytes 8388608 | tf_op jit(solution)/shard_map/stack | solution.py:149
  154.3 15.8 %reduce-scatter.11.cloned.1.call-done = bf16[32,1024]{1,0:T(8,128)(2,1)} async-done(((bf16[128,1024]{1,0:T(8,128)(2,1)}), bf16[32,1024]{1,0:T(8,128)(2,1)}) %reduce-scatter.11.cloned.1.call-update) | async-done | bytes 65552 | tf_op jit(solution)/shard_map/reduce_scatter | solution.py:144
  170.1 1.5 add_convert_fusion
  (84 shorter events, 4.9 us)
Async XLA Ops:
  7.2 1.9 %copy-start.6 = (bf16[32,1024]{1,0:T(8,128)(2,1)S(1)}, bf16[32,1024]{1,0:T(8,128)(2,1)}, u32[]{:S(2)}) copy-start(bf16[32,1024]{1,0:T(8,128)(2,1)} %param.13) | copy-start | bytes 196612
  7.2 17.7 %copy-start.8 = (f32[2,1024]{1,0:T(2,128)S(1)}, f32[2,1024]{1,0:T(2,128)}, u32[]{:S(2)}) copy-start(f32[2,1024]{1,0:T(2,128)} %param.15) | copy-start | bytes 24580
  7.2 53.4 %reduce-scatter.5.cloned.1.call-start = ((), (), s32[]{:S(2)}) async-start(), calls=%async_computation.4 | async-start | bytes 1146880 | tf_op jit(solution)/shard_map/reduce_scatter | solution.py:91
  7.2 17.7 %copy-start.4 = (bf16[2,1024,512]{2,1,0:T(8,128)(2,1)S(1)}, bf16[2,1024,512]{2,1,0:T(8,128)(2,1)}, u32[]{:S(2)}) copy-start(bf16[2,1024,512]{2,1,0:T(8,128)(2,1)} %param.17) | copy-start | bytes 6291460
  7.2 17.8 %copy-start.5 = (bf16[2,1024,512]{2,1,0:T(8,128)(2,1)S(1)}, bf16[2,1024,512]{2,1,0:T(8,128)(2,1)}, u32[]{:S(2)}) copy-start(bf16[2,1024,512]{2,1,0:T(8,128)(2,1)} %param.18) | copy-start | bytes 6291460
  24.9 2.2 %copy-start.2 = (bf16[2,1024,1024]{2,1,0:T(8,128)(2,1)S(1)}, bf16[2,1024,1024]{2,1,0:T(8,128)(2,1)}, u32[]{:S(2)}) copy-start(bf16[2,1024,1024]{2,1,0:T(8,128)(2,1)} %param.19) | copy-start | bytes 12582916
  27.1 2.2 %copy-start.3 = (bf16[2,1024,1024]{2,1,0:T(8,128)(2,1)S(1)}, bf16[2,1024,1024]{2,1,0:T(8,128)(2,1)}, u32[]{:S(2)}) copy-start(bf16[2,1024,1024]{2,1,0:T(8,128)(2,1)} %param.20) | copy-start | bytes 12582916
  29.7 3.0 %copy-start = (bf16[1024,3584]{1,0:T(8,128)(2,1)}, bf16[1024,3584]{1,0:T(8,128)(2,1)S(1)}, u32[]{:S(2)}) copy-start(bf16[1024,3584]{1,0:T(8,128)(2,1)S(1)} %get-tuple-element.3) | copy-start | bytes 22020100
  32.7 2.2 %copy-start.14 = (u32[32]{0:T(128)S(1)}, u32[32]{0:T(128)}, u32[]{:S(2)}) copy-start(u32[32]{0:T(128)} %constant.34) | copy-start | bytes 388
  32.7 3.4 %copy-start.13 = (s32[2]{0:T(128)S(1)}, s32[2]{0:T(128)}, u32[]{:S(2)}) copy-start(s32[2]{0:T(128)} %param.14) | copy-start | bytes 28
  32.7 9.5 %copy-start.9 = (f32[2,512]{1,0:T(2,128)S(1)}, f32[2,512]{1,0:T(2,128)}, u32[]{:S(2)}) copy-start(f32[2,512]{1,0:T(2,128)} %param.21) | copy-start | bytes 12292
  32.7 9.5 %copy-start.10 = (f32[2,512]{1,0:T(2,128)S(1)}, f32[2,512]{1,0:T(2,128)}, u32[]{:S(2)}) copy-start(f32[2,512]{1,0:T(2,128)} %param.23) | copy-start | bytes 12292
  34.8 60.0 %reduce-scatter.7.cloned.1.call-start = ((), (), s32[]{:S(2)}) async-start(), calls=%async_computation.5 | async-start | bytes 327680 | tf_op jit(solution)/shard_map/reduce_scatter | solution.py:144
  42.2 19.4 %copy-start.7 = (f32[2,32,512]{2,1,0:T(8,128)S(1)}, f32[2,32,512]{2,1,0:T(8,128)}, u32[]{:S(2)}) copy-start(f32[2,32,512]{2,1,0:T(8,128)} %param.22) | copy-start | bytes 393220
  62.1 11.4 %copy-start.11 = (bf16[2,1024,1024]{2,1,0:T(8,128)(2,1)S(1)}, bf16[2,1024,1024]{2,1,0:T(8,128)(2,1)}, u32[]{:S(2)}) copy-start(bf16[2,1024,1024]{2,1,0:T(8,128)(2,1)} %param.24) | copy-start | bytes 12582916
  74.6 62.8 %reduce-scatter.9.cloned.1.call-start = ((), (), s32[]{:S(2)}) async-start(), calls=%async_computation.6 | async-start | bytes 1146880 | tf_op jit(solution)/shard_map/reduce_scatter | solution.py:91
  114.8 55.2 %reduce-scatter.11.cloned.1.call-start = ((), (), s32[]{:S(2)}) async-start(), calls=%async_computation.7 | async-start | bytes 327680 | tf_op jit(solution)/shard_map/reduce_scatter | solution.py:144
  139.0 9.7 %copy-start.12 = (bf16[2,1024,1024]{2,1,0:T(8,128)(2,1)S(1)}, bf16[2,1024,1024]{2,1,0:T(8,128)(2,1)}, u32[]{:S(2)}) copy-start(bf16[2,1024,1024]{2,1,0:T(8,128)(2,1)} %param.24) | copy-start | bytes 12582916
  149.9 1.9 %copy-start.1 = (f32[2,2,256,512]{3,2,1,0:T(8,128)S(1)}, f32[2,2,256,512]{3,2,1,0:T(8,128)}, u32[]{:S(2)}) copy-start(f32[2,2,256,512]{3,2,1,0:T(8,128)} %multiply_add_fusion.1) | copy-start | bytes 6291460
Sparse Core Ops, SparseCore 0:
  34.9 25.5 reduce-scatter.4
  74.8 20.0 reduce-scatter.6
  115.0 22.4 reduce-scatter.8
  150.0 19.9 reduce-scatter.10
where the time goes:
time: 179 us; the launch traced here: 178 us
  waiting for transfers between devices  61.7 us (34%)
  blocking collectives  52.8 us (29%)
  matrix products  22.8 us (13%)
  local copies, waits for them, and re-layouts  15.4 us (9%)
  between operations  14.9 us (8%)
  other arithmetic  10.3 us (6%)
    reduce_scatter x2, waiting for transfers between devices, local(): lax.psum_scatter(partials.astype(jnp.bfloat16), 'tp', scatter_dimension=0...  35.9 us
    all_gather x2, blocking collectives, local(): gathered = lax.all_gather(current, 'tp', axis=0, tiled=True)  29.8 us
    reduce_scatter x2, waiting for transfers between devices, local(): lax.psum_scatter(jnp.dot(scaled, joined, preferred_element_type=jnp.float...  25.7 us
    all_gather x2, blocking collectives, local(): lax.all_gather(gated, 'dp', axis=0, tiled=True)  11.5 us
    unnamed x2, blocking collectives  11.5 us
    unnamed x37, local copies, waits for them, and re-layouts  9.81 us
    dot_general x2, matrix products, local(): jnp.dot(scaled, joined, preferred_element_type=jnp.float32)  7.26 us
    dot_general x2, matrix products, recurrence(): jnp.einsum('sjhk,sjhv->shkv', weighted, values_in, precision=HIGH)  6.71 us
  transfers between devices with their start and end apart: 4, of which 4 were waited for; matrix products, arithmetic and copies ran while one was open for 8% of the time, Pallas kernels for 0%

commit v1 on v0

--- a/solution.py
+++ b/solution.py
@@ -1,6 +1,10 @@
+import functools
+
 import jax
 import jax.numpy as jnp
 from jax import lax
+from jax.experimental import pallas as pl
+from jax.experimental.pallas import tpu as pltpu
 from jax.sharding import PartitionSpec as P
 
 D = 4096
@@ -149,6 +153,499 @@
     return (current, jnp.stack(outputs))
 
 
+MESH = pl.DeviceIdType.MESH
+LAYERS = 2
+SEQS = 2
+HIDDEN = -1e30
+
+
+def fused_kernel(
+    n_tp,
+    stream,
+    lengths,
+    gain_in,
+    wq_in,
+    wk_in,
+    wf_in,
+    wv_in,
+    wg_in,
+    bias_in,
+    extra_in,
+    hgain_in,
+    wo_in,
+    memory_in,
+    stream_out,
+    memory_out,
+    w,
+    wo,
+    mem,
+    fresh,
+    gain,
+    bias,
+    extra,
+    hgain,
+    ag,
+    xs,
+    pb,
+    r1,
+    s2,
+    r2,
+    sq_s,
+    sq_r,
+    gbuf,
+    rs_s,
+    rs_r,
+    w_sem,
+    wo_sem,
+    mem_sem,
+    out_sem,
+    small_sem,
+    ag_ss,
+    ag_rs,
+    p1_ss,
+    p1_rs,
+    p2_ss,
+    p2_rs,
+    sq_ss,
+    sq_rs,
+    g_ss,
+    g_rs,
+    o_ss,
+    o_rs,
+):
+    tp = lax.axis_index("tp")
+    dp = lax.axis_index("dp")
+    chip = dp // 2
+    core = dp % 2
+    rows = stream.shape[0]
+    chunk = w.shape[3]
+    chunks = w.shape[1]
+    key_local = wq_in.shape[2]
+    value_local = wv_in.shape[2]
+    heads = key_local // KEY_DIM
+    own = rows
+
+    dp_peers = [chip * 2 + 1 - core, (1 - chip) * 2 + core, (1 - chip) * 2 + 1 - core]
+    tp_offsets = list(range(1, n_tp))
+
+    def tp_to(offset):
+        return lax.rem(tp + offset, n_tp)
+
+    def tp_from(offset):
+        return lax.rem(tp + n_tp - offset, n_tp)
+
+    first = pltpu.make_async_copy(stream, ag.at[0, tp], small_sem.at[0])
+    first.start()
+    gain_copy = pltpu.make_async_copy(gain_in, gain, small_sem.at[1])
+    gain_copy.start()
+
+    def weight_copies(l):
+        pieces = []
+        for source in (wq_in, wk_in, wf_in, wv_in, wg_in):
+            for at in range(0, source.shape[2], chunk):
+                pieces.append(source.at[l, :, pl.ds(at, chunk)])
+        return [
+            pltpu.make_async_copy(piece, w.at[l, c], w_sem.at[l, c])
+            for c, piece in enumerate(pieces)
+        ]
+
+    for copy in weight_copies(0):
+        copy.start()
+
+    barrier = pltpu.get_barrier_semaphore()
+    for offset in tp_offsets:
+        pl.semaphore_signal(barrier, inc=1, device_id={"tp": tp_to(offset)}, device_id_type=MESH)
+    for peer in dp_peers:
+        pl.semaphore_signal(barrier, inc=1, device_id={"dp": peer}, device_id_type=MESH)
+    others = [
+        pltpu.make_async_copy(bias_in, bias, small_sem.at[2]),
+        pltpu.make_async_copy(extra_in, extra, small_sem.at[3]),
+        pltpu.make_async_copy(hgain_in, hgain, small_sem.at[4]),
+    ]
+    for copy in others:
+        copy.start()
+    pl.semaphore_wait(barrier, len(tp_offsets) + len(dp_peers))
+    first.wait()
+    gain_copy.wait()
+    for copy in others:
+        copy.wait()
+
+    row_of = lax.broadcasted_iota(jnp.int32, (own, 1), 0)
+    seq_of = row_of // BLOCK_LEN
+    place = row_of - seq_of * BLOCK_LEN
+    live_count = jnp.where(seq_of == 0, lengths[0], lengths[1])
+    alive = jnp.where(place < live_count, 1.0, 0.0).astype(jnp.float32)
+    lane = lax.broadcasted_iota(jnp.int32, (own, 128), 1)
+
+    def mem_copy(l):
+        return pltpu.make_async_copy(memory_in.at[l], mem.at[l], mem_sem.at[l])
+
+    def wo_copy(l):
+        return pltpu.make_async_copy(wo_in.at[l], wo.at[l], wo_sem.at[l])
+
+    def fresh_copy(l):
+        return pltpu.make_async_copy(fresh.at[l], memory_out.at[l], out_sem.at[l])
+
+    def layer(l, carry):
+        gather = []
+        for offset in tp_offsets:
+            copy = pltpu.make_async_remote_copy(
+                src_ref=ag.at[l, tp],
+                dst_ref=ag.at[l, tp],
+                send_sem=ag_ss.at[l, offset],
+                recv_sem=ag_rs.at[l, offset],
+                device_id={"tp": tp_to(offset)},
+                device_id_type=MESH,
+            )
+            copy.start()
+            gather.append(copy)
+        gain_row = gain[pl.ds(l, 1), :]
+        diag = lax.broadcasted_iota(jnp.int32, (own, 128), 0)
+
+        def prepare(source):
+            wide = ag[l, source].astype(jnp.float32)
+            xs[pl.ds(source * rows, rows), :] = (wide * gain_row).astype(jnp.bfloat16)
+            power = jnp.sum(wide * wide, axis=1, keepdims=True)
+            return jnp.sum(jnp.where(lane == diag + source * rows, power, 0.0), axis=0, keepdims=True)
+
+        powers = prepare(tp)
+        for offset in tp_offsets:
+            pltpu.make_async_remote_copy(
+                src_ref=ag.at[l, tp],
+                dst_ref=ag.at[l, tp_from(offset)],
+                send_sem=ag_ss.at[l, offset],
+                recv_sem=ag_rs.at[l, offset],
+                device_id={"tp": tp_to(offset)},
+                device_id_type=MESH,
+            ).wait_recv()
+            powers = powers + prepare(tp_from(offset))
+        sq_s[l] = jnp.broadcast_to(powers, (8, 128))
+
+        @pl.when(l == 0)
+        def _():
+            mem_copy(0).start()
+            wo_copy(0).start()
+
+        def stage_one(c):
+            return pltpu.make_async_remote_copy(
+                src_ref=pb.at[l, c, :, 1 - core],
+                dst_ref=r1.at[l, c],
+                send_sem=p1_ss.at[l, c],
+                recv_sem=p1_rs.at[l, c],
+                device_id={"dp": dp_peers[0]},
+                device_id_type=MESH,
+            )
+
+        def stage_two(c):
+            return pltpu.make_async_remote_copy(
+                src_ref=s2.at[l, c],
+                dst_ref=r2.at[l, c],
+                send_sem=p2_ss.at[l, c],
+                recv_sem=p2_rs.at[l, c],
+                device_id={"dp": dp_peers[1]},
+                device_id_type=MESH,
+            )
+
+        def pass_on(c):
+            stage_one(c).wait_recv()
+            s2[l, c] = (
+                pb[l, c, 1 - chip, core].astype(jnp.float32)
+                + r1[l, c, 1 - chip].astype(jnp.float32)
+            ).astype(jnp.bfloat16)
+            stage_two(c).start()
+
+        squares = []
+        weights = weight_copies(l)
+        for c in range(chunks):
+            weights[c].wait()
+            part = jnp.dot(xs[...], w[l, c], preferred_element_type=jnp.float32)
+            pb[l, c] = part.astype(jnp.bfloat16).reshape(2, 2, rows, chunk)
+            stage_one(c).start()
+            if c == 0:
+                for k, peer in enumerate(dp_peers):
+                    copy = pltpu.make_async_remote_copy(
+                        src_ref=sq_s.at[l],
+                        dst_ref=sq_r.at[l, k],
+                        send_sem=sq_ss.at[l, k],
+                        recv_sem=sq_rs.at[l, k],
+                        device_id={"dp": peer},
+                        device_id_type=MESH,
+                    )
+                    copy.start()
+                    squares.append(copy)
+            else:
+                pass_on(c - 1)
+        pass_on(chunks - 1)
+
+        @pl.when(l == 0)
+        def _():
+            for copy in weight_copies(1):
+                copy.start()
+            mem_copy(1).start()
+            wo_copy(1).start()
+
+        total = sq_s[l]
+        for k in range(len(dp_peers)):
+            squares[k].wait_recv()
+            total = total + sq_r[l, k]
+        own_power = jnp.sum(
+            jnp.where(lane == diag + dp * own, total[0:1, :], 0.0), axis=1, keepdims=True
+        )
+        row_scale = lax.rsqrt(own_power / D + EPS)
+
+        def summed(c):
+            stage_two(c).wait_recv()
+            both = pb[l, c, chip, core].astype(jnp.float32) + r1[l, c, chip].astype(jnp.float32)
+            return (both + r2[l, c].astype(jnp.float32)) * row_scale
+
+        key_chunks = key_local // chunk
+        value_chunks = value_local // chunk
+
+        def taken(start, count):
+            parts = [summed(c) for c in range(start, start + count)]
+            return parts[0] if count == 1 else jnp.concatenate(parts, axis=1)
+
+        queries = taken(0, key_chunks) * KEY_DIM ** (-0.5)
+        keys_in = taken(key_chunks, key_chunks) * alive
+        forget = taken(2 * key_chunks, key_chunks) + bias[pl.ds(l, 1), :]
+        log_sig = jnp.minimum(forget, 0.0) - jnp.log(1.0 + jnp.exp(-jnp.abs(forget)))
+        totals = (log_sig / TIME_CONSTANT + extra[l]) * alive
+        step = 1
+        while step < BLOCK_LEN:
+            totals = totals + jnp.where(place >= step, pltpu.roll(totals, step, 0), 0.0)
+            step *= 2
+
+        def each_seq(array, j):
+            return jnp.concatenate(
+                [
+                    jnp.broadcast_to(
+                        array[s * BLOCK_LEN + j : s * BLOCK_LEN + j + 1, :],
+                        (BLOCK_LEN, array.shape[1]),
+                    )
+                    for s in range(SEQS)
+                ],
+                axis=0,
+            )
+
+        scores = [jnp.zeros((own, 128), jnp.float32) for _ in range(heads)]
+        for j in range(BLOCK_LEN):
+            decay = jnp.exp(jnp.where(place >= j, totals - each_seq(totals, j), HIDDEN))
+            product = queries * decay * each_seq(keys_in, j)
+            for h in range(heads):
+                column = jnp.sum(
+                    product[:, h * KEY_DIM : (h + 1) * KEY_DIM], axis=1, keepdims=True
+                )
+                scores[h] = jnp.where(lane == seq_of * BLOCK_LEN + j, column, scores[h])
+        carried_q = (queries * jnp.exp(totals)).astype(jnp.bfloat16)
+        last = each_seq(totals, BLOCK_LEN - 1)
+        weighted = (keys_in * jnp.exp(last - totals)).astype(jnp.bfloat16)
+        last_decay = jnp.exp(last)
+
+        mem_copy(l).wait()
+        carried = []
+        for h in range(heads):
+            span = slice(h * KEY_DIM, (h + 1) * KEY_DIM)
+            carried.append(
+                jnp.concatenate(
+                    [
+                        jnp.dot(
+                            carried_q[s * BLOCK_LEN : (s + 1) * BLOCK_LEN, span],
+                            mem[l, s, span, :].astype(jnp.bfloat16),
+                            preferred_element_type=jnp.float32,
+                        )
+                        for s in range(SEQS)
+                    ],
+                    axis=0,
+                )
+            )
+        values_in = taken(3 * key_chunks, value_chunks).astype(jnp.bfloat16)
+        normed = []
+        for h in range(heads):
+            read = carried[h] + jnp.dot(
+                scores[h][:, :own].astype(jnp.bfloat16),
+                values_in[:, h * VALUE_DIM : (h + 1) * VALUE_DIM],
+                preferred_element_type=jnp.float32,
+            )
+            normed.append(
+                read
+                * lax.rsqrt(jnp.mean(read * read, axis=1, keepdims=True) + EPS)
+                * hgain[pl.ds(l, 1), :]
+            )
+        gate_pre = taken(3 * key_chunks + value_chunks, value_chunks)
+        flat = jnp.concatenate(normed, axis=1)
+        gbuf[l, dp] = (flat * (gate_pre * jax.nn.sigmoid(gate_pre)) * alive).astype(jnp.bfloat16)
+
+        def gated_copy(k, source):
+            return pltpu.make_async_remote_copy(
+                src_ref=gbuf.at[l, dp],
+                dst_ref=gbuf.at[l, source],
+                send_sem=g_ss.at[l, k],
+                recv_sem=g_rs.at[l, k],
+                device_id={"dp": dp_peers[k]},
+                device_id_type=MESH,
+            )
+
+        for k in (1, 2, 0):
+            gated_copy(k, dp).start()
+
+        def partial_copy(dest):
+            return pltpu.make_async_remote_copy(
+                src_ref=rs_s.at[l, dest],
+                dst_ref=rs_r.at[l, tp],
+                send_sem=o_ss.at[l, dest],
+                recv_sem=o_rs.at[l, tp],
+                device_id={"tp": dest},
+                device_id_type=MESH,
+            )
+
+        def project(side):
+            left = gbuf[l, pl.ds(2 * side, 2)].reshape(2 * rows, value_local)
+            out = jnp.dot(left, wo[l], preferred_element_type=jnp.float32)
+            rs_s[l, pl.ds(2 * side, 2)] = out.astype(jnp.bfloat16).reshape(2, rows, out.shape[1])
+            for i in range(2):
+                dest = 2 * side + i
+
+                @pl.when(dest != tp)
+                def _():
+                    partial_copy(dest).start()
+
+        def update(s, h):
+            span = slice(h * KEY_DIM, (h + 1) * KEY_DIM)
+            ahead = slice(s * BLOCK_LEN, (s + 1) * BLOCK_LEN)
+            grown = lax.dot_general(
+                weighted[ahead, span],
+                values_in[ahead, h * VALUE_DIM : (h + 1) * VALUE_DIM],
+                (((0,), (0,)), ((), ())),
+                preferred_element_type=jnp.float32,
+            )
+            kept = jnp.transpose(
+                jnp.broadcast_to(last_decay[s * BLOCK_LEN : s * BLOCK_LEN + 1, span], (128, KEY_DIM))
+            )
+            kept = jnp.concatenate([kept] * (VALUE_DIM // 128), axis=1)
+            fresh[l, s, span, :] = kept * mem[l, s, span, :] + grown
+
+        wo_copy(l).wait()
+        gated_copy(0, dp_peers[0]).wait_recv()
+        project(chip)
+        for s in range(SEQS):
+            for h in range(heads):
+                update(s, h)
+        fresh_copy(l).start()
+        gated_copy(1, dp_peers[1]).wait_recv()
+        gated_copy(2, dp_peers[2]).wait_recv()
+        project(1 - chip)
+
+        mixed = rs_s[l, tp].astype(jnp.float32)
+        for offset in tp_offsets:
+            source = tp_from(offset)
+            pltpu.make_async_remote_copy(
+                src_ref=rs_s.at[l, source],
+                dst_ref=rs_r.at[l, source],
+                send_sem=o_ss.at[l, source],
+                recv_sem=o_rs.at[l, source],
+                device_id={"tp": source},
+                device_id_type=MESH,
+            ).wait_recv()
+            mixed = mixed + rs_r[l, source].astype(jnp.float32)
+        mixed = mixed.astype(jnp.bfloat16).astype(jnp.float32)
+        ag[l + 1, tp] = (ag[l, tp].astype(jnp.float32) + mixed).astype(jnp.bfloat16)
+
+        for copy in gather + squares:
+            copy.wait_send()
+        for c in range(chunks):
+            stage_one(c).wait_send()
+            stage_two(c).wait_send()
+        for k in range(len(dp_peers)):
+            gated_copy(k, dp).wait_send()
+        for offset in tp_offsets:
+            partial_copy(tp_to(offset)).wait_send()
+        return carry
+
+    lax.fori_loop(0, LAYERS, layer, 0)
+    done = pltpu.make_async_copy(ag.at[LAYERS, tp], stream_out, small_sem.at[0])
+    done.start()
+    for l in range(LAYERS):
+        fresh_copy(l).wait()
+    done.wait()
+
+
+def fused(n_tp, *args):
+    stream, wq, wv, wo_all, memory = args[0], args[3], args[6], args[11], args[12]
+    rows, features = stream.shape
+    key_local, value_local = wq.shape[2], wv.shape[2]
+    chunk = KEY_DIM * 2
+    chunks = (3 * key_local + 2 * value_local) // chunk
+    n_dp = 4
+    bf, f32 = jnp.bfloat16, jnp.float32
+    dma = pltpu.SemaphoreType.DMA
+    anywhere = pl.BlockSpec(memory_space=pl.ANY)
+    in_specs = [anywhere] * len(args)
+    in_specs[1] = pl.BlockSpec(memory_space=pltpu.SMEM)
+    return pl.pallas_call(
+        functools.partial(fused_kernel, n_tp),
+        out_shape=(
+            jax.ShapeDtypeStruct(stream.shape, bf),
+            jax.ShapeDtypeStruct(memory.shape, f32),
+        ),
+        in_specs=in_specs,
+        out_specs=(anywhere, anywhere),
+        scratch_shapes=[
+            pltpu.VMEM((LAYERS, chunks, features, chunk), bf),
+            pltpu.VMEM(wo_all.shape, bf),
+            pltpu.VMEM(memory.shape, f32),
+            pltpu.VMEM(memory.shape, f32),
+            pltpu.VMEM(args[2].shape, f32),
+            pltpu.VMEM(args[8].shape, f32),
+            pltpu.VMEM(args[9].shape, f32),
+            pltpu.VMEM(args[10].shape, f32),
+            pltpu.VMEM((LAYERS + 1, n_tp, rows, features), bf),
+            pltpu.VMEM((n_tp * rows, features), bf),
+            pltpu.VMEM((LAYERS, chunks, 2, 2, rows, chunk), bf),
+            pltpu.VMEM((LAYERS, chunks, 2, rows, chunk), bf),
+            pltpu.VMEM((LAYERS, chunks, rows, chunk), bf),
+            pltpu.VMEM((LAYERS, chunks, rows, chunk), bf),
+            pltpu.VMEM((LAYERS, 8, 128), f32),
+            pltpu.VMEM((LAYERS, n_dp - 1, 8, 128), f32),
+            pltpu.VMEM((LAYERS, n_dp, rows, value_local), bf),
+            pltpu.VMEM((LAYERS, n_tp, rows, features), bf),
+            pltpu.VMEM((LAYERS, n_tp, rows, features), bf),
+            dma((LAYERS, chunks)),
+            dma((LAYERS,)),
+            dma((LAYERS,)),
+            dma((LAYERS,)),
+            dma((5,)),
+            dma((LAYERS, n_tp)),
+            dma((LAYERS, n_tp)),
+            dma((LAYERS, chunks)),
+            dma((LAYERS, chunks)),
+            dma((LAYERS, chunks)),
+            dma((LAYERS, chunks)),
+            dma((LAYERS, n_dp - 1)),
+            dma((LAYERS, n_dp - 1)),
+            dma((LAYERS, n_dp - 1)),
+            dma((LAYERS, n_dp - 1)),
+            dma((LAYERS, n_tp)),
+            dma((LAYERS, n_tp)),
+        ],
+        compiler_params=pltpu.CompilerParams(
+            collective_id=0, has_side_effects=True, vmem_limit_bytes=60 * 1024 * 1024
+        ),
+    )(*args)
+
+
+def body(*args):
+    stream, wq = args[0], args[3]
+    n_tp, n_dp = lax.axis_size("tp"), lax.axis_size("dp")
+    fits = (
+        n_dp == 4
+        and n_tp == 4
+        and args[1].shape[0] == SEQS
+        and stream.shape[0] == SEQS * BLOCK_LEN
+        and wq.shape[2] % (2 * KEY_DIM) == 0
+    )
+    return fused(n_tp, *args) if fits else local(*args)
+
+
 def solution(mesh):
     placed = (
         P(("grp", "tp"), "dp"),
@@ -166,7 +663,7 @@
         P(None, ("grp", "dp"), "tp", None),
     )
     return jax.shard_map(
-        local,
+        body,
         mesh=mesh,
         in_specs=placed,
         out_specs=(P(("grp", "tp"), "dp"), P(None, ("grp", "dp"), "tp", None)),

time: 179 us -> 70 us (0.39)
  the two profiles are of different devices: /device:TPU:0 before, /device:TPU:25 now
where the time goes in v1:
time: 70 us; the launch traced here: 69.8 us
  Pallas kernels  63 us (90%)
  local copies, waits for them, and re-layouts  6.11 us (9%)
    pallas_call x1, Pallas kernels, fused(): pl.pallas_call(functools.partial(fused_kernel, n_tp), out_shape=(jax.Shap...  63 us
    unnamed x2, local copies, waits for them, and re-layouts  6.11 us

profile of v1, /device:TPU:25, one launch (start us, length us, event | category | flops | bytes accessed | tf_op | source)
XLA Modules:
  0.0 69.8 jit_solution(11986407330048232055)
XLA Ops:
  0.6 63.0 %shard_map.140 = (bf16[32,1024]{1,0:T(8,128)(2,1)}, f32[2,2,512,512]{3,2,1,0:T(8,128)}) custom-call(bf16[32,1024]{1,0:T(8,128)(2,1)} %stream.1, s32[2]{0:T(128)} %lengths.1, f32[2,1024]{1,0:T(2,128)} %gain_in.1, bf16[2,1024,512]{2,1,0:T(8,128)(2,1)} %wq_in.1, bf16[2,1024,512]{2,1,0:T(8,128)(2,1)} %wk_in.1, bf16[2,1024,512]{2,1,0:T(8,128)(2,1)} %wf_in.1, ...), custom_call_target="tpu_custom_call" | custom-call | tf_op jit(solution)/shard_map/pallas_call | solution.py:584
  63.7 1.5 %copy.17 = bf16[32,1024]{1,0:T(8,128)(2,1)} copy(bf16[32,1024]{1,0:T(8,128)(2,1)} %get-tuple-element.4) | data formatting | bytes 131072
  65.1 4.6 %copy.18 = f32[2,2,512,512]{3,2,1,0:T(8,128)} copy(f32[2,2,512,512]{3,2,1,0:T(8,128)} %get-tuple-element.5) | data formatting | bytes 8388608

commit v2 on v1

--- a/solution.py
+++ b/solution.py
@@ -156,6 +156,8 @@
 MESH = pl.DeviceIdType.MESH
 LAYERS = 2
 SEQS = 2
+PARTS = 2
+LAG = 4
 HIDDEN = -1e30
 
 
@@ -200,6 +202,7 @@
     mem_sem,
     out_sem,
     small_sem,
+    stream_sem,
     ag_ss,
     ag_rs,
     p1_ss,
@@ -224,6 +227,8 @@
     value_local = wv_in.shape[2]
     heads = key_local // KEY_DIM
     own = rows
+    parts = ag.shape[1]
+    width = ag.shape[4]
 
     dp_peers = [chip * 2 + 1 - core, (1 - chip) * 2 + core, (1 - chip) * 2 + 1 - core]
     tp_offsets = list(range(1, n_tp))
@@ -234,8 +239,13 @@
     def tp_from(offset):
         return lax.rem(tp + n_tp - offset, n_tp)
 
-    first = pltpu.make_async_copy(stream, ag.at[0, tp], small_sem.at[0])
-    first.start()
+    def stream_copy(b):
+        return pltpu.make_async_copy(
+            stream.at[:, pl.ds(b * width, width)], ag.at[0, b, tp], stream_sem.at[b]
+        )
+
+    for b in range(parts):
+        stream_copy(b).start()
     gain_copy = pltpu.make_async_copy(gain_in, gain, small_sem.at[1])
     gain_copy.start()
 
@@ -249,26 +259,39 @@
             for c, piece in enumerate(pieces)
         ]
 
-    for copy in weight_copies(0):
-        copy.start()
+    others = [
+        pltpu.make_async_copy(bias_in, bias, small_sem.at[2]),
+        pltpu.make_async_copy(extra_in, extra, small_sem.at[3]),
+        pltpu.make_async_copy(hgain_in, hgain, small_sem.at[4]),
+    ]
 
     barrier = pltpu.get_barrier_semaphore()
     for offset in tp_offsets:
         pl.semaphore_signal(barrier, inc=1, device_id={"tp": tp_to(offset)}, device_id_type=MESH)
     for peer in dp_peers:
         pl.semaphore_signal(barrier, inc=1, device_id={"dp": peer}, device_id_type=MESH)
-    others = [
-        pltpu.make_async_copy(bias_in, bias, small_sem.at[2]),
-        pltpu.make_async_copy(extra_in, extra, small_sem.at[3]),
-        pltpu.make_async_copy(hgain_in, hgain, small_sem.at[4]),
-    ]
-    for copy in others:
+    for copy in weight_copies(0) + others:
         copy.start()
     pl.semaphore_wait(barrier, len(tp_offsets) + len(dp_peers))
-    first.wait()
+
+    def gather_copy(l, b, offset, source):
+        return pltpu.make_async_remote_copy(
+            src_ref=ag.at[l, b, tp],
+            dst_ref=ag.at[l, b, source],
+            send_sem=ag_ss.at[l, b, offset],
+            recv_sem=ag_rs.at[l, b, offset],
+            device_id={"tp": tp_to(offset)},
+            device_id_type=MESH,
+        )
+
+    def gather_start(l, b):
+        for offset in tp_offsets:
+            gather_copy(l, b, offset, tp).start()
+
+    for b in range(parts):
+        stream_copy(b).wait()
+        gather_start(0, b)
     gain_copy.wait()
-    for copy in others:
-        copy.wait()
 
     row_of = lax.broadcasted_iota(jnp.int32, (own, 1), 0)
     seq_of = row_of // BLOCK_LEN
@@ -287,38 +310,25 @@
         return pltpu.make_async_copy(fresh.at[l], memory_out.at[l], out_sem.at[l])
 
     def layer(l, carry):
-        gather = []
-        for offset in tp_offsets:
-            copy = pltpu.make_async_remote_copy(
-                src_ref=ag.at[l, tp],
-                dst_ref=ag.at[l, tp],
-                send_sem=ag_ss.at[l, offset],
-                recv_sem=ag_rs.at[l, offset],
-                device_id={"tp": tp_to(offset)},
-                device_id_type=MESH,
-            )
-            copy.start()
-            gather.append(copy)
         gain_row = gain[pl.ds(l, 1), :]
         diag = lax.broadcasted_iota(jnp.int32, (own, 128), 0)
 
-        def prepare(source):
-            wide = ag[l, source].astype(jnp.float32)
-            xs[pl.ds(source * rows, rows), :] = (wide * gain_row).astype(jnp.bfloat16)
+        def prepare(b, source):
+            columns = slice(b * width, (b + 1) * width)
+            wide = ag[l, b, source].astype(jnp.float32)
+            xs[pl.ds(source * rows, rows), columns] = (wide * gain_row[:, columns]).astype(
+                jnp.bfloat16
+            )
             power = jnp.sum(wide * wide, axis=1, keepdims=True)
             return jnp.sum(jnp.where(lane == diag + source * rows, power, 0.0), axis=0, keepdims=True)
 
-        powers = prepare(tp)
-        for offset in tp_offsets:
-            pltpu.make_async_remote_copy(
-                src_ref=ag.at[l, tp],
-                dst_ref=ag.at[l, tp_from(offset)],
-                send_sem=ag_ss.at[l, offset],
-                recv_sem=ag_rs.at[l, offset],
-                device_id={"tp": tp_to(offset)},
-                device_id_type=MESH,
-            ).wait_recv()
-            powers = powers + prepare(tp_from(offset))
+        powers = jnp.zeros((1, 128), jnp.float32)
+        for b in range(parts):
+            powers = powers + prepare(b, tp)
+        for b in range(parts):
+            for offset in tp_offsets:
+                gather_copy(l, b, offset, tp_from(offset)).wait_recv()
+                powers = powers + prepare(b, tp_from(offset))
         sq_s[l] = jnp.broadcast_to(powers, (8, 128))
 
         @pl.when(l == 0)
@@ -373,9 +383,10 @@
                     )
                     copy.start()
                     squares.append(copy)
-            else:
-                pass_on(c - 1)
-        pass_on(chunks - 1)
+            if c >= LAG:
+                pass_on(c - LAG)
+        for c in range(max(0, chunks - LAG), chunks):
+            pass_on(c)
 
         @pl.when(l == 0)
         def _():
@@ -383,6 +394,11 @@
                 copy.start()
             mem_copy(1).start()
             wo_copy(1).start()
+
+        @pl.when(l == 0)
+        def _():
+            for copy in others:
+                copy.wait()
 
         total = sq_s[l]
         for k in range(len(dp_peers)):
@@ -488,26 +504,28 @@
         for k in (1, 2, 0):
             gated_copy(k, dp).start()
 
-        def partial_copy(dest):
+        def partial_copy(b, dest, source):
             return pltpu.make_async_remote_copy(
-                src_ref=rs_s.at[l, dest],
-                dst_ref=rs_r.at[l, tp],
-                send_sem=o_ss.at[l, dest],
-                recv_sem=o_rs.at[l, tp],
+                src_ref=rs_s.at[l, b, dest],
+                dst_ref=rs_r.at[l, b, source],
+                send_sem=o_ss.at[l, b, dest],
+                recv_sem=o_rs.at[l, b, source],
                 device_id={"tp": dest},
                 device_id_type=MESH,
             )
 
-        def project(side):
+        def project(side, b):
             left = gbuf[l, pl.ds(2 * side, 2)].reshape(2 * rows, value_local)
-            out = jnp.dot(left, wo[l], preferred_element_type=jnp.float32)
-            rs_s[l, pl.ds(2 * side, 2)] = out.astype(jnp.bfloat16).reshape(2, rows, out.shape[1])
+            out = jnp.dot(
+                left, wo[l, :, b * width : (b + 1) * width], preferred_element_type=jnp.float32
+            )
+            rs_s[l, b, pl.ds(2 * side, 2)] = out.astype(jnp.bfloat16).reshape(2, rows, width)
             for i in range(2):
                 dest = 2 * side + i
 
                 @pl.when(dest != tp)
                 def _():
-                    partial_copy(dest).start()
+                    partial_copy(b, dest, tp).start()
 
         def update(s, h):
             span = slice(h * KEY_DIM, (h + 1) * KEY_DIM)
@@ -522,51 +540,60 @@
                 jnp.broadcast_to(last_decay[s * BLOCK_LEN : s * BLOCK_LEN + 1, span], (128, KEY_DIM))
             )
             kept = jnp.concatenate([kept] * (VALUE_DIM // 128), axis=1)
-            fresh[l, s, span, :] = kept * mem[l, s, span, :] + grown
+            fresh[l, s, span, :] = (kept * mem[l, s, span, :] + grown).astype(jnp.bfloat16)
 
         wo_copy(l).wait()
         gated_copy(0, dp_peers[0]).wait_recv()
-        project(chip)
+        for b in range(parts):
+            project(chip, b)
         for s in range(SEQS):
             for h in range(heads):
                 update(s, h)
         fresh_copy(l).start()
         gated_copy(1, dp_peers[1]).wait_recv()
         gated_copy(2, dp_peers[2]).wait_recv()
-        project(1 - chip)
-
-        mixed = rs_s[l, tp].astype(jnp.float32)
-        for offset in tp_offsets:
-            source = tp_from(offset)
-            pltpu.make_async_remote_copy(
-                src_ref=rs_s.at[l, source],
-                dst_ref=rs_r.at[l, source],
-                send_sem=o_ss.at[l, source],
-                recv_sem=o_rs.at[l, source],
-                device_id={"tp": source},
-                device_id_type=MESH,
-            ).wait_recv()
-            mixed = mixed + rs_r[l, source].astype(jnp.float32)
-        mixed = mixed.astype(jnp.bfloat16).astype(jnp.float32)
-        ag[l + 1, tp] = (ag[l, tp].astype(jnp.float32) + mixed).astype(jnp.bfloat16)
-
-        for copy in gather + squares:
+        for b in range(parts):
+            project(1 - chip, b)
+
+        for b in range(parts):
+            mixed = rs_s[l, b, tp].astype(jnp.float32)
+            for offset in tp_offsets:
+                source = tp_from(offset)
+                partial_copy(b, source, source).wait_recv()
+                mixed = mixed + rs_r[l, b, source].astype(jnp.float32)
+            mixed = mixed.astype(jnp.bfloat16).astype(jnp.float32)
+            ag[l + 1, b, tp] = (ag[l, b, tp].astype(jnp.float32) + mixed).astype(jnp.bfloat16)
+
+            @pl.when(l + 1 < LAYERS)
+            def _():
+                gather_start(l + 1, b)
+
+        for copy in squares:
             copy.wait_send()
         for c in range(chunks):
             stage_one(c).wait_send()
             stage_two(c).wait_send()
         for k in range(len(dp_peers)):
             gated_copy(k, dp).wait_send()
-        for offset in tp_offsets:
-            partial_copy(tp_to(offset)).wait_send()
+        for b in range(parts):
+            for offset in tp_offsets:
+                gather_copy(l, b, offset, tp).wait_send()
+                partial_copy(b, tp_to(offset), tp).wait_send()
         return carry
 
     lax.fori_loop(0, LAYERS, layer, 0)
-    done = pltpu.make_async_copy(ag.at[LAYERS, tp], stream_out, small_sem.at[0])
-    done.start()
+    done = [
+        pltpu.make_async_copy(
+            ag.at[LAYERS, b, tp], stream_out.at[:, pl.ds(b * width, width)], stream_sem.at[b]
+        )
+        for b in range(parts)
+    ]
+    for copy in done:
+        copy.start()
     for l in range(LAYERS):
         fresh_copy(l).wait()
-    done.wait()
+    for copy in done:
+        copy.wait()
 
 
 def fused(n_tp, *args):
@@ -585,7 +612,7 @@
         functools.partial(fused_kernel, n_tp),
         out_shape=(
             jax.ShapeDtypeStruct(stream.shape, bf),
-            jax.ShapeDtypeStruct(memory.shape, f32),
+            jax.ShapeDtypeStruct(memory.shape, bf),
         ),
         in_specs=in_specs,
         out_specs=(anywhere, anywhere),
@@ -593,12 +620,12 @@
             pltpu.VMEM((LAYERS, chunks, features, chunk), bf),
             pltpu.VMEM(wo_all.shape, bf),
             pltpu.VMEM(memory.shape, f32),
-            pltpu.VMEM(memory.shape, f32),
+            pltpu.VMEM(memory.shape, bf),
             pltpu.VMEM(args[2].shape, f32),
             pltpu.VMEM(args[8].shape, f32),
             pltpu.VMEM(args[9].shape, f32),
             pltpu.VMEM(args[10].shape, f32),
-            pltpu.VMEM((LAYERS + 1, n_tp, rows, features), bf),
+            pltpu.VMEM((LAYERS + 1, PARTS, n_tp, rows, features // PARTS), bf),
             pltpu.VMEM((n_tp * rows, features), bf),
             pltpu.VMEM((LAYERS, chunks, 2, 2, rows, chunk), bf),
             pltpu.VMEM((LAYERS, chunks, 2, rows, chunk), bf),
@@ -607,15 +634,16 @@
             pltpu.VMEM((LAYERS, 8, 128), f32),
             pltpu.VMEM((LAYERS, n_dp - 1, 8, 128), f32),
             pltpu.VMEM((LAYERS, n_dp, rows, value_local), bf),
-            pltpu.VMEM((LAYERS, n_tp, rows, features), bf),
-            pltpu.VMEM((LAYERS, n_tp, rows, features), bf),
+            pltpu.VMEM((LAYERS, PARTS, n_tp, rows, features // PARTS), bf),
+            pltpu.VMEM((LAYERS, PARTS, n_tp, rows, features // PARTS), bf),
             dma((LAYERS, chunks)),
             dma((LAYERS,)),
             dma((LAYERS,)),
             dma((LAYERS,)),
             dma((5,)),
-            dma((LAYERS, n_tp)),
-            dma((LAYERS, n_tp)),
+            dma((PARTS,)),
+            dma((LAYERS, PARTS, n_tp)),
+            dma((LAYERS, PARTS, n_tp)),
             dma((LAYERS, chunks)),
             dma((LAYERS, chunks)),
             dma((LAYERS, chunks)),
@@ -624,8 +652,8 @@
             dma((LAYERS, n_dp - 1)),
             dma((LAYERS, n_dp - 1)),
             dma((LAYERS, n_dp - 1)),
-            dma((LAYERS, n_tp)),
-            dma((LAYERS, n_tp)),
+            dma((LAYERS, PARTS, n_tp)),
+            dma((LAYERS, PARTS, n_tp)),
         ],
         compiler_params=pltpu.CompilerParams(
             collective_id=0, has_side_effects=True, vmem_limit_bytes=60 * 1024 * 1024
@@ -643,7 +671,10 @@
         and stream.shape[0] == SEQS * BLOCK_LEN
         and wq.shape[2] % (2 * KEY_DIM) == 0
     )
-    return fused(n_tp, *args) if fits else local(*args)
+    if not fits:
+        return local(*args)
+    current, memories = fused(n_tp, *args)
+    return current, memories.astype(jnp.float32)
 
 
 def solution(mesh):

time: 70 us -> 66.3 us (0.947)
  local copies, waits for them, and re-layouts: 6.11 us -> 0.63 us
  other arithmetic: 0 us -> 4.22 us
  Pallas kernels: 63 us -> 60.1 us
    unnamed x2 -> x3, local copies, waits for them, and re-layouts: 6.11 us -> 0.63 us
    convert_element_type x0 -> x1, other arithmetic: none -> 4.22 us  [body(): return (current, memories.astype(jnp.float32))]
    pallas_call x1, Pallas kernels: 63 us -> 60.1 us  [fused(): pl.pallas_call(functools.partial(fused_kernel, n_tp), out_shape=(jax.Shap...]
where the time goes in v2:
time: 66.3 us; the launch traced here: 65.6 us
  Pallas kernels  60.1 us (91%)
  other arithmetic  4.22 us (6%)
    pallas_call x1, Pallas kernels, fused(): pl.pallas_call(functools.partial(fused_kernel, n_tp), out_shape=(jax.Shap...  60.1 us
    convert_element_type x1, other arithmetic, body(): return (current, memories.astype(jnp.float32))  4.22 us

profile of v2, /device:TPU:25, one launch (start us, length us, event | category | flops | bytes accessed | tf_op | source)
XLA Modules:
  0.0 65.6 jit_solution(11591111950161865300)
XLA Ops:
  0.6 60.1 %shard_map.140 = (bf16[32,1024]{1,0:T(8,128)(2,1)}, bf16[2,2,512,512]{3,2,1,0:T(8,128)(2,1)}) custom-call(bf16[32,1024]{1,0:T(8,128)(2,1)} %stream.1, s32[2]{0:T(128)} %lengths.1, f32[2,1024]{1,0:T(2,128)} %gain_in.1, bf16[2,1024,512]{2,1,0:T(8,128)(2,1)} %wq_in.1, bf16[2,1024,512]{2,1,0:T(8,128)(2,1)} %wk_in.1, bf16[2,1024,512]{2,1,0:T(8,128)(2,1)} %wf_in.1, ...), custom_call_target="tpu_custom_call" | custom-call | tf_op jit(solution)/shard_map/pallas_call | solution.py:611
  60.7 0.0 copy-start
  60.7 4.2 %convert_element_type.3 = f32[2,2,512,512]{3,2,1,0:T(8,128)} convert(bf16[2,2,512,512]{3,2,1,0:T(8,128)(2,1)} %get-tuple-element.5) | non-fusion elementwise | flops 1048576 | bytes 6291456 | tf_op jit(solution)/shard_map/convert_element_type | solution.py:677
  65.0 0.0 copy-done
  65.0 0.6 copy.16
Async XLA Ops:
  60.7 4.2 %copy-start = (bf16[32,1024]{1,0:T(8,128)(2,1)S(1)}, bf16[32,1024]{1,0:T(8,128)(2,1)}, u32[]{:S(2)}) copy-start(bf16[32,1024]{1,0:T(8,128)(2,1)} %get-tuple-element.8) | copy-start | bytes 196612
